TPU v7x, 32 devices: a whole 2x2x4 slice. The times are simulated.
32 devices in a mesh: ep: 8 (over z, y), tp: 4 (over x, core).
Axes of the slice: x: 2, y: 2, z: 4, core: 2. Of those that a mesh axis runs over, the one named last changes fastest.
Arguments:
- tokens: bfloat16 [1024, 2048], P('ep', 'tp'), may hold values from -6 to 6
- norm_gain: bfloat16 [2048], P('tp'), may hold values from 0.099609375 to 1.8984375
- routes: int32 [1024, 2], P('ep'), may hold values from 0 to 7, as said below
- gate_weights: float32 [1024, 2], P('ep'), may hold values from 0.1 to 1
- w_gate: bfloat16 [8, 2048, 4096], P('ep', None, 'tp'), may hold values from -0.125 to 0.125
- w_up: bfloat16 [8, 2048, 4096], P('ep', None, 'tp'), may hold values from -0.125 to 0.125
- w_down: bfloat16 [8, 4096, 2048], P('ep', 'tp'), may hold values from -0.875 to 0.875
- out_gain: bfloat16 [2048], P('tp'), may hold values from 0.099609375 to 1.8984375
Outputs:
- mixed: bfloat16 [1024, 2048], P('ep', 'tp')
Inputs may be any that keep to these rules, and one draw needn't show every extreme that they name: `routes`: each row names 2 different experts of one group (their quotients by 8 agree). In each aligned block of 128 rows no expert is named by more than 64 rows, and in every block some expert is named by exactly 64 rows.
All inputs are finite; a program needn't handle non-finite values.
Results may differ from a plain program's by a relative error of at most 0.019.
Values may be sent and summed in bfloat16 or wider, within the bound.
A program may use at most 64 MiB of HBM per device.

v0:
```python
import jax
import jax.numpy as jnp
from jax import lax
from jax.sharding import PartitionSpec as P

epsilon = 1e-06


def shards(tokens, norm_gain, routes, gate_weights, w_gate, w_up, w_down, out_gain):
    tok_rows = tokens.shape[0]
    width_local = tokens.shape[1]
    full_width = width_local * lax.axis_size("tp")
    experts = lax.axis_size("ep")
    top_count = routes.shape[1]
    capacity = 2 * top_count * tok_rows // experts
    flat_ids = routes.reshape(-1)
    onehot = (flat_ids[:, None] == jnp.arange(experts, dtype=jnp.int32)[None, :]).astype(jnp.int32)
    before = jnp.cumsum(onehot, axis=0) - onehot
    slot_index = jnp.sum(before * onehot, axis=1)
    dest_index = flat_ids * capacity + slot_index
    dest_pairs = dest_index.reshape(tok_rows, top_count)
    places = jnp.arange(experts * capacity, dtype=jnp.int32)
    scatter_mat = jnp.any(dest_pairs[None, :, :] == places[:, None, None], axis=2).astype(
        jnp.bfloat16
    )
    gate_mat = w_gate[0]
    up_mat = w_up[0]
    x_float = tokens.astype(jnp.float32)
    row_sums = lax.psum(jnp.sum(x_float * x_float, axis=1), "tp")
    scale_in = lax.rsqrt(row_sums / full_width + epsilon)
    normed = (x_float * scale_in[:, None] * norm_gain.astype(jnp.float32)).astype(jnp.bfloat16)
    outgoing = jnp.dot(scatter_mat, normed, preferred_element_type=jnp.float32).astype(jnp.bfloat16)
    arrived = lax.all_to_all(outgoing, "ep", split_axis=0, concat_axis=0, tiled=True)
    portion = lax.all_gather(arrived, "tp", axis=1, tiled=True)
    gate_sum = jnp.dot(portion, gate_mat, preferred_element_type=jnp.float32)
    up_sum = jnp.dot(portion, up_mat, preferred_element_type=jnp.float32)
    hidden = (jax.nn.silu(gate_sum) * up_sum).astype(jnp.bfloat16)
    down_mat = w_down[0]
    summed = lax.psum_scatter(
        lax.dot_general(
            down_mat, hidden, (((0,), (1,)), ((), ())), preferred_element_type=jnp.float32
        ).astype(jnp.bfloat16),
        "tp",
        scatter_dimension=0,
        tiled=True,
    )
    came_back = lax.all_to_all(summed, "ep", split_axis=1, concat_axis=1, tiled=True)
    picked = (
        jnp.take(came_back, dest_index, axis=1)
        .astype(jnp.float32)
        .reshape(width_local, tok_rows, top_count)
    )
    combined = jnp.sum(picked * gate_weights[None, :, :], axis=2).T
    out_sums = lax.psum(jnp.sum(combined * combined, axis=1), "tp")
    scale_out = lax.rsqrt(out_sums / full_width + epsilon)
    return (combined * scale_out[:, None] * out_gain.astype(jnp.float32)).astype(jnp.bfloat16)


def solution(mesh):
    placed = (
        P("ep", "tp"),
        P("tp"),
        P("ep", None),
        P("ep", None),
        P("ep", None, "tp"),
        P("ep", None, "tp"),
        P("ep", "tp", None),
        P("tp"),
    )
    return jax.shard_map(
        shards, mesh=mesh, in_specs=placed, out_specs=P("ep", "tp"), check_vma=False
    )
```

profile of v0, /device:TPU:0, one launch (start us, length us, event | category | flops | bytes accessed | tf_op | source)
XLA Modules:
  0.0 145.3 jit_solution(15379768702945613426)
XLA Ops:
  6.5 0.8 copy.21
  7.3 0.1 eq.39
  7.5 0.1 reshape.77
  7.6 0.6 reduce-window.6
  8.2 0.2 slice_reduce_fusion
  8.6 0.1 reduce_sum.41
  8.8 0.7 compare_and_fusion
  9.5 0.7 convert_element_type.45
  10.2 1.0 fusion.17
  11.2 8.4 %psum.14 = f32[128]{0:T(128)S(1)} all-reduce(f32[128]{0:T(128)S(1)} %fusion.17), channel_id=1, replica_groups=mesh['ep'=8,'tp'=4] {'tp'}, use_global_device_ids=true, to_apply=%region_5.6 | all-reduce | flops 128 | bytes 1024 | tf_op jit(solution)/shard_map/psum | solution.py:29
  19.6 1.3 convolution_convert_fusion
  20.9 19.0 %all_to_all.24 = bf16[8,64,512]{2,1,0:T(8,128)(2,1)} all-to-all(bf16[8,64,512]{2,1,0:T(8,128)(2,1)S(1)} %bitcast.43), channel_id=1, replica_groups=mesh['ep'=8,'tp'=4] {'ep'}, dimensions={0} | all-to-all | bytes 1048576 | tf_op jit(solution)/shard_map/all_to_all | solution.py:33
  40.0 21.8 %all-gather.2.cloned.1.call-done = bf16[512,2048]{1,0:T(8,128)(2,1)} async-done(((bf16[512,512]{1,0:T(8,128)(2,1)}), bf16[512,2048]{1,0:T(8,128)(2,1)}) %all-gather.2.cloned.1.call-update) | async-done | bytes 2097168 | tf_op jit(solution)/shard_map/all_gather | solution.py:34
  61.7 6.6 %fusion.4 = f32[512,1024]{1,0:T(8,128)} fusion(bf16[512,2048]{1,0:T(8,128)(2,1)} %all-gather.2.cloned.1.call-done, bf16[1,2048,1024]{2,1,0:T(8,128)(2,1)} %param.12), kind=kOutput, calls=%fused_computation.5 | convolution fusion | flops 2147483648 | bytes 8388608 | tf_op jit(solution)/shard_map/dot_general | solution.py:35
  68.3 10.0 %fusion.9 = bf16[2048,512]{0,1:T(8,128)(2,1)} fusion(bf16[1,1024,2048]{2,1,0:T(8,128)(2,1)} %param.14, f32[512,1024]{1,0:T(8,128)} %fusion.4, bf16[512,2048]{1,0:T(8,128)(2,1)S(1)} %copy-done.3, bf16[1,2048,1024]{2,1,0:T(8,128)(2,1)} %param.13), kind=kOutput, calls=%fused_computation.8 | convolution fusion | flops 4299161600 | bytes 14680064 | tf_op jit(solution)/shard_map/dot_general | solution.py:40
  78.4 31.3 %reduce-scatter.2.cloned.1.call-done = bf16[512,512]{0,1:T(8,128)(2,1)} async-done(((bf16[2048,512]{0,1:T(8,128)(2,1)}), bf16[512,512]{0,1:T(8,128)(2,1)}) %reduce-scatter.2.cloned.1.call-update) | async-done | bytes 524304 | tf_op jit(solution)/shard_map/reduce_scatter | solution.py:39
  109.7 5.5 %all-to-all-start.1 = ((bf16[512,8,64]{0,2,1:T(8,128)(2,1)}), bf16[512,8,64]{0,2,1:T(8,128)(2,1)S(1)}, u32[]{:S(2)}, u32[]{:S(2)}) async-start(bf16[512,8,64]{0,2,1:T(8,128)(2,1)} %bitcast.45), calls=%async_computation.2 | async-start | bytes 1048576 | tf_op jit(solution)/shard_map/all_to_all | solution.py:47
  115.4 0.1 mul.90
  115.5 0.1 copy.24
  115.8 13.7 %all-to-all-done.1 = bf16[512,8,64]{0,2,1:T(8,128)(2,1)S(1)} async-done(((bf16[512,8,64]{0,2,1:T(8,128)(2,1)}), bf16[512,8,64]{0,2,1:T(8,128)(2,1)S(1)}, u32[]{:S(2)}, u32[]{:S(2)}) %all-to-all-start.1) | async-done | bytes 524320 | tf_op jit(solution)/shard_map/all_to_all | solution.py:47
  129.5 1.2 gather_fusion
  130.8 0.8 multiply_reduce_fusion
  131.8 6.0 %psum.15 = f32[128]{0:T(128)S(1)} all-reduce(f32[128]{0:T(128)S(1)} %multiply_reduce_fusion.1), channel_id=1, replica_groups=mesh['ep'=8,'tp'=4] {'tp'}, use_global_device_ids=true, to_apply=%region_9.10 | all-reduce | flops 128 | bytes 1024 | tf_op jit(solution)/shard_map/psum | solution.py:54
  137.7 0.8 fusion.20
  (28 shorter events, 0.8 us)
Async XLA Ops:
  6.5 55.2 %all-gather.2.cloned.1.call-start = ((), (), s32[]{:S(2)}) async-start(), calls=%async_computation.3 | async-start | bytes 2621440 | tf_op jit(solution)/shard_map/all_gather | solution.py:34
  39.9 69.8 %reduce-scatter.2.cloned.1.call-start = ((), (), s32[]{:S(2)}) async-start(), calls=%async_computation.4 | async-start | bytes 2621440 | tf_op jit(solution)/shard_map/reduce_scatter | solution.py:39
  61.7 6.6 %copy-start.3 = (bf16[512,2048]{1,0:T(8,128)(2,1)S(1)}, bf16[512,2048]{1,0:T(8,128)(2,1)}, u32[]{:S(2)}) copy-start(bf16[512,2048]{1,0:T(8,128)(2,1)} %all-gather.2.cloned.1.call-done) | copy-start | bytes 6291460
  78.3 36.9 %copy-start = (s32[128,2]{0,1:T(2,128)S(1)}, s32[128,2]{0,1:T(2,128)}, u32[]{:S(2)}) copy-start(s32[128,2]{0,1:T(2,128)} %param.10) | copy-start | bytes 3076
  78.3 37.3 %copy-start.1 = (f32[128,2]{0,1:T(2,128)S(1)}, f32[128,2]{0,1:T(2,128)}, u32[]{:S(2)}) copy-start(f32[128,2]{0,1:T(2,128)} %param.11) | copy-start | bytes 3076
  78.3 37.4 %copy-start.2 = (bf16[512]{0:T(512)(128)(2,1)S(1)}, bf16[512]{0:T(512)(128)(2,1)}, u32[]{:S(2)}) copy-start(bf16[512]{0:T(512)(128)(2,1)} %param.15) | copy-start | bytes 3076
  109.7 19.8 %all-to-all-start.1 = ((bf16[512,8,64]{0,2,1:T(8,128)(2,1)}), bf16[512,8,64]{0,2,1:T(8,128)(2,1)S(1)}, u32[]{:S(2)}, u32[]{:S(2)}) async-start(bf16[512,8,64]{0,2,1:T(8,128)(2,1)} %bitcast.45), calls=%async_computation.2 | async-start | bytes 1048576 | tf_op jit(solution)/shard_map/all_to_all | solution.py:47
Sparse Core Ops, SparseCore 0:
  40.1 21.6 all-gather.1
  78.5 31.1 reduce-scatter.1
where the time goes:
time: 146 us; the launch traced here: 145 us
  waiting for transfers between devices  66.9 us (46%)
  blocking collectives  33.3 us (23%)
  matrix products  17.9 us (12%)
  between operations  13.5 us (9%)
  starting transfers between devices  5.56 us (4%)
  other arithmetic  4.93 us (3%)
  local copies, waits for them, and re-layouts  3.25 us (2%)
    reduce_scatter x1, waiting for transfers between devices, shards(): lax.psum_scatter(lax.dot_general(down_mat, hidden, (((0,), (1,)), ((), ()...  31.3 us
    all_gather x1, waiting for transfers between devices, shards(): portion = lax.all_gather(arrived, 'tp', axis=1, tiled=True)  21.8 us
    all_to_all x1, blocking collectives, shards(): lax.all_to_all(outgoing, 'ep', split_axis=0, concat_axis=0, tiled=True)  19 us
    all_to_all x1, waiting for transfers between devices, shards(): lax.all_to_all(summed, 'ep', split_axis=1, concat_axis=1, tiled=True)  13.7 us
    dot_general x1, matrix products, shards(): lax.dot_general(down_mat, hidden, (((0,), (1,)), ((), ())), preferred_ele...  10 us
    psum x1, blocking collectives, shards(): row_sums = lax.psum(jnp.sum(x_float * x_float, axis=1), 'tp')  8.37 us
    dot_general x1, matrix products, shards(): gate_sum = jnp.dot(portion, gate_mat, preferred_element_type=jnp.float32)  6.59 us
    psum x1, blocking collectives, shards(): out_sums = lax.psum(jnp.sum(combined * combined, axis=1), 'tp')  5.95 us
  transfers between devices with their start and end apart: 3, of which 3 were waited for; matrix products, arithmetic and copies ran while one was open for 0% of the time, Pallas kernels for 0%

commit v1 on v0

--- a/solution.py
+++ b/solution.py
@@ -1,9 +1,14 @@
+import functools
+
 import jax
 import jax.numpy as jnp
 from jax import lax
+from jax.experimental import pallas as pl
+from jax.experimental.pallas import tpu as pltpu
 from jax.sharding import PartitionSpec as P
 
 epsilon = 1e-06
+CORES = 2
 
 
 def shards(tokens, norm_gain, routes, gate_weights, w_gate, w_up, w_down, out_gain):
@@ -56,6 +61,315 @@
     return (combined * scale_out[:, None] * out_gain.astype(jnp.float32)).astype(jnp.bfloat16)
 
 
+def xor(index, mask):
+    result = index
+    bit = 1
+    while bit <= mask:
+        if mask & bit:
+            result = result + bit * (1 - 2 * ((index // bit) % 2))
+        bit *= 2
+    return result
+
+
+def layer(
+    n_ep, cap, near,
+    routes_ref, gates_ref, tokens_ref, in_gain_ref, out_gain_ref, wg_hbm, wu_hbm, wd_hbm,
+    out_ref,
+    wg, wu, wd, picked, xall, gains, xn, hidden, psend, prec, own, xsend, xrec, rsend, back, sums,
+    w_sem, disp_s, disp_r, part_s, part_r, opp_s, opp_r, rel_s, rel_r, gain_s, gain_r,
+    pd_s, pd_r, xs_s, xs_r, ret_s, ret_r, ns_s, ns_r,
+):
+    f32, bf16 = jnp.float32, jnp.bfloat16
+    ep, tp = lax.axis_index("ep"), lax.axis_index("tp")
+    chip, core = tp // CORES, tp % CORES
+    partner = chip * CORES + (1 - core)
+    opposite = (1 - chip) * CORES + core
+    diagonal = (1 - chip) * CORES + (1 - core)
+    tok, width = tokens_ref.shape
+    n_tp = gains.shape[0]
+    full = width * n_tp
+    ff = wg.shape[1]
+    half_rows = n_ep // 2 * cap
+    source = [xor(ep, d) for d in range(n_ep)]
+    rows = [pl.ds(pl.multiple_of(s * cap, cap), cap) for s in source]
+    my_rows = rows[0]
+
+    barrier = pltpu.get_barrier_semaphore()
+    for d in range(1, n_ep):
+        pl.semaphore_signal(barrier, inc=1, device_id={"ep": source[d]})
+    for peer in (partner, opposite, diagonal):
+        pl.semaphore_signal(barrier, inc=1, device_id={"tp": peer})
+
+    weights = [
+        pltpu.make_async_copy(src.at[0], dst, w_sem.at[i])
+        for i, (src, dst) in enumerate(((wg_hbm, wg), (wu_hbm, wu), (wd_hbm, wd)))
+    ]
+    for copy in weights:
+        copy.start()
+
+    def remote(src, dst, send, recv, where):
+        return pltpu.make_async_remote_copy(
+            src_ref=src, dst_ref=dst, send_sem=send, recv_sem=recv, device_id=where
+        )
+
+    routes = routes_ref[...]
+    first, second = routes[:, 0:1], routes[:, 1:2]
+    lanes = 128 * pl.cdiv(n_ep, 128)
+    expert = lax.broadcasted_iota(jnp.int32, (tok, lanes), 1)
+    is_first, is_second = expert == first, expert == second
+    member = jnp.where(is_first, 1.0, 0.0) + jnp.where(is_second, 1.0, 0.0)
+    earlier = jnp.where(
+        lax.broadcasted_iota(jnp.int32, (tok, tok), 1)
+        < lax.broadcasted_iota(jnp.int32, (tok, tok), 0),
+        1.0,
+        0.0,
+    )
+    before = jnp.dot(earlier.astype(bf16), member.astype(bf16), preferred_element_type=f32)
+    place = before + (expert * cap).astype(f32)
+    place_first = jnp.sum(jnp.where(is_first, place, 0.0), axis=1, keepdims=True)
+    place_second = jnp.sum(jnp.where(is_second, place, 0.0), axis=1, keepdims=True)
+    slots = lax.broadcasted_iota(jnp.int32, (tok, n_ep * cap), 1).astype(f32)
+    at_first, at_second = slots == place_first, slots == place_second
+    select = (jnp.where(at_first, 1.0, 0.0) + jnp.where(at_second, 1.0, 0.0)).astype(bf16)
+    picked[...] = lax.dot_general(
+        select, tokens_ref[...], (((0,), (0,)), ((), ())), preferred_element_type=f32
+    ).astype(bf16)
+    gains[pl.ds(tp, 1)] = in_gain_ref[...].astype(f32)[None]
+    xall[pl.ds(tp, 1), my_rows] = picked[my_rows][None]
+
+    pl.semaphore_wait(barrier, n_ep - 1 + n_tp - 1)
+
+    dispatch = {
+        d: remote(picked.at[rows[d]], xall.at[tp, my_rows], disp_s.at[d], disp_r.at[d], {"ep": source[d]})
+        for d in range(1, n_ep)
+    }
+    to_partner, to_opposite, relay = [], [], []
+    for d in range(n_ep):
+        block = xall.at[tp, rows[d]]
+        to_partner.append(remote(block, block, part_s.at[d], part_r.at[d], {"tp": partner}))
+        to_opposite.append(remote(block, block, opp_s.at[d], opp_r.at[d], {"tp": opposite}))
+        far = xall.at[opposite, rows[d]]
+        relay.append(remote(far, far, rel_s.at[d], rel_r.at[d], {"tp": partner}))
+    gain_copies = [
+        remote(gains.at[tp], gains.at[tp], gain_s.at[i], gain_r.at[i], {"tp": peer})
+        for i, peer in enumerate((partner, opposite, diagonal))
+    ]
+    for copy in gain_copies:
+        copy.start()
+    to_opposite[0].start()
+    to_partner[0].start()
+    order = near[1:]
+    for d in order:
+        dispatch[d].start()
+
+    def forward(d):
+        dispatch[d].wait_recv()
+        to_opposite[d].start()
+        to_partner[d].start()
+
+    def pass_on(d):
+        to_opposite[d].wait_recv()
+        relay[d].start()
+
+    def normalise(i, d):
+        to_partner[d].wait_recv()
+        relay[d].wait_recv()
+        parts = [xall[j, rows[d]].astype(f32) for j in range(n_tp)]
+        total = sum(jnp.sum(p * p, axis=1, keepdims=True) for p in parts)
+        scale = lax.rsqrt(total / full + epsilon)
+        for j in range(n_tp):
+            xn[i * cap : (i + 1) * cap, j * width : (j + 1) * width] = (
+                parts[j] * scale * gains[j]
+            ).astype(bf16)
+
+    tile = min(256, ff)
+    tiles = ff // tile
+
+    def units(h, start, stop):
+        mine = slice(h * half_rows, (h + 1) * half_rows)
+
+        def body(n, carry):
+            cols = pl.ds(pl.multiple_of(n * tile, tile), tile)
+            gate = jnp.dot(xn[mine], wg[:, cols], preferred_element_type=f32)
+            up = jnp.dot(xn[mine], wu[:, cols], preferred_element_type=f32)
+            hidden[mine, cols] = (gate / (1.0 + jnp.exp(-gate)) * up).astype(bf16)
+            return carry
+
+        lax.fori_loop(start, stop, body, 0)
+
+    far_partner, near_partner = diagonal, partner
+    partner_copies = {
+        (h, k): remote(psend.at[h, k], prec.at[h, k], pd_s.at[h, k], pd_r.at[h, k], {"tp": partner})
+        for h in range(2)
+        for k in range(2)
+    }
+
+    def down(h):
+        mine = slice(h * half_rows, (h + 1) * half_rows)
+
+        def product(j):
+            cols = pl.ds(pl.multiple_of(j * width, width), width)
+            return jnp.dot(hidden[mine], wd[:, cols], preferred_element_type=f32)
+
+        for k, j in enumerate((far_partner, near_partner)):
+            psend[h, k] = product(j).astype(bf16)
+            partner_copies[h, k].start()
+        for k, j in enumerate((opposite, tp)):
+            own[h, k] = product(j)
+
+    across = [
+        remote(xsend.at[i], xrec.at[i], xs_s.at[i], xs_r.at[i], {"tp": opposite})
+        for i in range(n_ep)
+    ]
+    returned = {
+        d: remote(rsend.at[d], back.at[my_rows], ret_s.at[d], ret_r.at[d], {"ep": source[d]})
+        for d in range(1, n_ep)
+    }
+
+    def send_across(h):
+        partner_copies[h, 0].wait_recv()
+        for q in range(n_ep // 2):
+            i = h * (n_ep // 2) + q
+            part = slice(q * cap, (q + 1) * cap)
+            xsend[i] = (own[h, 0, part] + prec[h, 0, part].astype(f32)).astype(bf16)
+            across[i].start()
+
+    def send_back(h):
+        partner_copies[h, 1].wait_recv()
+        for q in range(n_ep // 2):
+            i = h * (n_ep // 2) + q
+            d = near[i]
+            part = slice(q * cap, (q + 1) * cap)
+            both = own[h, 1, part] + prec[h, 1, part].astype(f32)
+            across[i].wait_recv()
+            done = (both + xrec[i].astype(f32)).astype(bf16)
+            if d == 0:
+                back[my_rows] = done
+            else:
+                rsend[d] = done
+                returned[d].start()
+
+    half = n_ep // 2
+    group_a, group_b = near[:half], near[half:]
+    for copy in gain_copies:
+        copy.wait_recv()
+    for i in range(1, half):
+        forward(group_a[i])
+        pass_on(group_a[i - 1])
+    pass_on(group_a[half - 1])
+    for i, d in enumerate(group_a):
+        normalise(i, d)
+    for copy in weights[:2]:
+        copy.wait()
+    pieces = min(half, tiles)
+    done = 0
+    for piece in range(pieces):
+        until = (piece + 1) * half // pieces
+        for i in range(done, until):
+            forward(group_b[i])
+            if i:
+                pass_on(group_b[i - 1])
+        done = until
+        units(0, piece * tiles // pieces, (piece + 1) * tiles // pieces)
+    pass_on(group_b[half - 1])
+    weights[2].wait()
+    down(0)
+    send_across(0)
+    for i, d in enumerate(group_b):
+        normalise(half + i, d)
+    units(1, 0, tiles)
+    send_back(0)
+    down(1)
+    send_across(1)
+    send_back(1)
+
+    gates = gates_ref[...]
+    mixing = jnp.where(at_first, gates[:, 0:1], 0.0) + jnp.where(at_second, gates[:, 1:2], 0.0)
+    high = mixing.astype(bf16)
+    low = (mixing - high.astype(f32)).astype(bf16)
+    for d in range(1, n_ep):
+        returned[d].wait_recv()
+    rows_back = back[...]
+    combined = jnp.dot(high, rows_back, preferred_element_type=f32) + jnp.dot(
+        low, rows_back, preferred_element_type=f32
+    )
+    diag = lax.broadcasted_iota(jnp.int32, (tok, tok), 0) == lax.broadcasted_iota(
+        jnp.int32, (tok, tok), 1
+    )
+    row_sum = jnp.sum(combined * combined, axis=1, keepdims=True)
+    flat = jnp.sum(jnp.where(diag, row_sum, 0.0), axis=0, keepdims=True)
+    sums[pl.ds(tp, 1)] = flat[None]
+    norm_copies = [
+        remote(sums.at[tp], sums.at[tp], ns_s.at[i], ns_r.at[i], {"tp": peer})
+        for i, peer in enumerate((partner, opposite, diagonal))
+    ]
+    for copy in norm_copies:
+        copy.start()
+
+    for copy in gain_copies + to_partner + to_opposite + relay + across:
+        copy.wait_send()
+    for copies in (dispatch, partner_copies, returned):
+        for copy in copies.values():
+            copy.wait_send()
+
+    for copy in norm_copies:
+        copy.wait()
+    total = sum(sums[j] for j in range(n_tp))
+    column = jnp.sum(jnp.where(diag, total, 0.0), axis=1, keepdims=True)
+    scale = lax.rsqrt(column / full + epsilon)
+    out_ref[...] = (combined * scale * out_gain_ref[...].astype(f32)).astype(bf16)
+
+
+def fused(tokens, norm_gain, routes, gate_weights, w_gate, w_up, w_down, out_gain):
+    n_ep, n_tp = lax.axis_size("ep"), lax.axis_size("tp")
+    tok, width = tokens.shape
+    cap = 2 * routes.shape[1] * tok // n_ep
+    _, d_model, ff = w_gate.shape
+    half_rows = n_ep // 2 * cap
+    near = (0, 2, 3, 1) + tuple(range(4, n_ep))
+    bf16, f32 = jnp.bfloat16, jnp.float32
+    dma = pltpu.SemaphoreType.DMA
+    vmem = pl.BlockSpec(memory_space=pltpu.VMEM)
+    anywhere = pl.BlockSpec(memory_space=pl.ANY)
+    slots = n_ep * cap
+    return pl.pallas_call(
+        functools.partial(layer, n_ep, cap, near),
+        out_shape=jax.ShapeDtypeStruct((tok, width), bf16),
+        in_specs=[vmem] * 5 + [anywhere] * 3,
+        out_specs=vmem,
+        scratch_shapes=[
+            pltpu.VMEM((d_model, ff), bf16),
+            pltpu.VMEM((d_model, ff), bf16),
+            pltpu.VMEM((ff, d_model), bf16),
+            pltpu.VMEM((slots, width), bf16),
+            pltpu.VMEM((n_tp, slots, width), bf16),
+            pltpu.VMEM((n_tp, 1, width), f32),
+            pltpu.VMEM((slots, d_model), bf16),
+            pltpu.VMEM((slots, ff), bf16),
+            pltpu.VMEM((2, 2, half_rows, width), bf16),
+            pltpu.VMEM((2, 2, half_rows, width), bf16),
+            pltpu.VMEM((2, 2, half_rows, width), f32),
+            pltpu.VMEM((n_ep, cap, width), bf16),
+            pltpu.VMEM((n_ep, cap, width), bf16),
+            pltpu.VMEM((n_ep, cap, width), bf16),
+            pltpu.VMEM((slots, width), bf16),
+            pltpu.VMEM((n_tp, 1, tok), f32),
+            dma((3,)),
+            *[dma((n_ep,))] * 8,
+            *[dma((3,))] * 2,
+            *[dma((2, 2))] * 2,
+            *[dma((n_ep,))] * 4,
+            *[dma((3,))] * 2,
+        ],
+        compiler_params=pltpu.CompilerParams(
+            collective_id=0, has_side_effects=True, vmem_limit_bytes=60 * 1024 * 1024
+        ),
+    )(
+        routes, gate_weights, tokens, norm_gain.reshape(1, -1), out_gain.reshape(1, -1),
+        w_gate, w_up, w_down,
+    )
+
+
 def solution(mesh):
     placed = (
         P("ep", "tp"),
@@ -67,6 +381,8 @@
         P("ep", "tp", None),
         P("tp"),
     )
+    n_ep = mesh.shape["ep"]
+    pairs = mesh.shape["tp"] == 2 * CORES and n_ep >= 8 and n_ep & (n_ep - 1) == 0
     return jax.shard_map(
-        shards, mesh=mesh, in_specs=placed, out_specs=P("ep", "tp"), check_vma=False
-    )
+        fused if pairs else shards, mesh=mesh, in_specs=placed, out_specs=P("ep", "tp"), check_vma=False
+    )

time: 146 us -> 65.9 us (0.45)
  waiting for transfers between devices: 66.9 us -> 0 us
  Pallas kernels: 0 us -> 58.1 us
  blocking collectives: 33.3 us -> 0 us
  matrix products: 17.9 us -> 0 us
  between operations: 13.5 us -> 0.01 us
  starting transfers between devices: 5.56 us -> 0 us
  other arithmetic: 4.93 us -> 0 us
  local copies, waits for them, and re-layouts: 3.25 us -> 6.88 us
    pallas_call x0 -> x1, Pallas kernels: none -> 58.1 us  [fused(): pl.pallas_call(functools.partial(layer, n_ep, cap, near), out_shape=jax.S...]
    reduce_scatter x1 -> x0, waiting for transfers between devices: 31.3 us -> none  [shards(): lax.psum_scatter(lax.dot_general(down_mat, hidden, (((0,), (1,)), ((), ()...]
    all_gather x1 -> x0, waiting for transfers between devices: 21.8 us -> none  [shards(): portion = lax.all_gather(arrived, 'tp', axis=1, tiled=True)]
    all_to_all x1 -> x0, blocking collectives: 19 us -> none  [shards(): lax.all_to_all(outgoing, 'ep', split_axis=0, concat_axis=0, tiled=True)]
    dot_general x3 -> x0, matrix products: 17.9 us -> none  [the longest x1 10 us: shards(): lax.dot_general(down_mat, hidden, (((0,), (1,)), ((), ())), preferred_ele...]
    psum x2 -> x0, blocking collectives: 14.3 us -> none  [the longest x1 8.37 us: shards(): row_sums = lax.psum(jnp.sum(x_float * x_float, axis=1), 'tp')]
    all_to_all x1 -> x0, waiting for transfers between devices: 13.7 us -> none  [shards(): lax.all_to_all(summed, 'ep', split_axis=1, concat_axis=1, tiled=True)]
    all_to_all x1 -> x0, starting transfers between devices: 5.51 us -> none  [shards(): lax.all_to_all(summed, 'ep', split_axis=1, concat_axis=1, tiled=True)]
  transfers between devices with their start and end apart: 3 -> 0, of which waited for: 3 -> 0; matrix products, arithmetic and copies ran while one was open for 0% -> 0% of each run, Pallas kernels for 0% -> 0%
where the time goes in v1:
time: 65.9 us; the launch traced here: 65 us
  Pallas kernels  58.1 us (88%)
  local copies, waits for them, and re-layouts  6.88 us (10%)
    pallas_call x1, Pallas kernels, fused(): pl.pallas_call(functools.partial(layer, n_ep, cap, near), out_shape=jax.S...  58.1 us
    unnamed x3, local copies, waits for them, and re-layouts  4.38 us

profile of v1, /device:TPU:0, one launch (start us, length us, event | category | flops | bytes accessed | tf_op | source)
XLA Modules:
  0.0 65.0 jit_solution(2959222718324228385)
XLA Ops:
  0.0 1.3 %reshape.6.in_gain_ref = bf16[1,512]{1,0:T(2,128)(2,1)} reshape(bf16[512]{0:T(512)(128)(2,1)} %param.9) | data formatting | bytes 2048 | tf_op jit(solution)/shard_map/reshape | solution.py:368
  1.3 1.2 %reshape.7.out_gain_ref = bf16[1,512]{1,0:T(2,128)(2,1)} reshape(bf16[512]{0:T(512)(128)(2,1)} %param.15) | data formatting | bytes 2048 | tf_op jit(solution)/shard_map/reshape | solution.py:368
  2.5 1.4 %copy.9.routes_ref = s32[128,2]{1,0:T(8,128)} copy(s32[128,2]{0,1:T(2,128)} %param.10) | data formatting | bytes 2048 | tf_op args[2]
  3.9 1.4 %copy.10.gates_ref = f32[128,2]{1,0:T(8,128)} copy(f32[128,2]{0,1:T(2,128)} %param.11) | data formatting | bytes 2048 | tf_op args[3]
  5.3 58.1 %shard_map.82 = bf16[128,512]{1,0:T(8,128)(2,1)} custom-call(s32[128,2]{1,0:T(8,128)} %copy.9.routes_ref, f32[128,2]{1,0:T(8,128)} %copy.10.gates_ref, bf16[128,512]{1,0:T(8,128)(2,1)} %tokens_ref.1, bf16[1,512]{1,0:T(2,128)(2,1)} %reshape.6.in_gain_ref, bf16[1,512]{1,0:T(2,128)(2,1)} %reshape.7.out_gain_ref, bf16[1,2048,1024]{2,1,0:T(8,128)(2,1)} %wg_hbm.1, ...), custom_call_target="tpu_custom_call" | custom-call | tf_op jit(solution)/shard_map/pallas_call | solution.py:335
  63.5 1.6 %copy.12 = bf16[128,512]{1,0:T(8,128)(2,1)} copy(bf16[128,512]{1,0:T(8,128)(2,1)} %shard_map.82) | data formatting | bytes 262144

commit v2 on v1

--- a/solution.py
+++ b/solution.py
@@ -112,10 +112,17 @@
             src_ref=src, dst_ref=dst, send_sem=send, recv_sem=recv, device_id=where
         )
 
-    routes = routes_ref[...]
-    first, second = routes[:, 0:1], routes[:, 1:2]
+    diag = lax.broadcasted_iota(jnp.int32, (tok, tok), 0) == lax.broadcasted_iota(
+        jnp.int32, (tok, tok), 1
+    )
+
+    def column(row):
+        return jnp.sum(jnp.where(diag, row, 0.0), axis=1, keepdims=True)
+
+    routes = routes_ref[...].astype(f32)
+    first, second = column(routes[0:1]), column(routes[1:2])
     lanes = 128 * pl.cdiv(n_ep, 128)
-    expert = lax.broadcasted_iota(jnp.int32, (tok, lanes), 1)
+    expert = lax.broadcasted_iota(jnp.int32, (tok, lanes), 1).astype(f32)
     is_first, is_second = expert == first, expert == second
     member = jnp.where(is_first, 1.0, 0.0) + jnp.where(is_second, 1.0, 0.0)
     earlier = jnp.where(
@@ -125,7 +132,7 @@
         0.0,
     )
     before = jnp.dot(earlier.astype(bf16), member.astype(bf16), preferred_element_type=f32)
-    place = before + (expert * cap).astype(f32)
+    place = before + expert * cap
     place_first = jnp.sum(jnp.where(is_first, place, 0.0), axis=1, keepdims=True)
     place_second = jnp.sum(jnp.where(is_second, place, 0.0), axis=1, keepdims=True)
     slots = lax.broadcasted_iota(jnp.int32, (tok, n_ep * cap), 1).astype(f32)
@@ -134,7 +141,7 @@
     picked[...] = lax.dot_general(
         select, tokens_ref[...], (((0,), (0,)), ((), ())), preferred_element_type=f32
     ).astype(bf16)
-    gains[pl.ds(tp, 1)] = in_gain_ref[...].astype(f32)[None]
+    gains[pl.ds(tp, 1)] = in_gain_ref[...].astype(f32).reshape(1, 1, width)
     xall[pl.ds(tp, 1), my_rows] = picked[my_rows][None]
 
     pl.semaphore_wait(barrier, n_ep - 1 + n_tp - 1)
@@ -234,20 +241,18 @@
             xsend[i] = (own[h, 0, part] + prec[h, 0, part].astype(f32)).astype(bf16)
             across[i].start()
 
-    def send_back(h):
-        partner_copies[h, 1].wait_recv()
-        for q in range(n_ep // 2):
-            i = h * (n_ep // 2) + q
-            d = near[i]
-            part = slice(q * cap, (q + 1) * cap)
-            both = own[h, 1, part] + prec[h, 1, part].astype(f32)
-            across[i].wait_recv()
-            done = (both + xrec[i].astype(f32)).astype(bf16)
-            if d == 0:
-                back[my_rows] = done
-            else:
-                rsend[d] = done
-                returned[d].start()
+    def send_back(i):
+        h, q = divmod(i, n_ep // 2)
+        d = near[i]
+        part = slice(q * cap, (q + 1) * cap)
+        both = own[h, 1, part] + prec[h, 1, part].astype(f32)
+        across[i].wait_recv()
+        done = (both + xrec[i].astype(f32)).astype(bf16)
+        if d == 0:
+            back[my_rows] = done
+        else:
+            rsend[d] = done
+            returned[d].start()
 
     half = n_ep // 2
     group_a, group_b = near[:half], near[half:]
@@ -277,14 +282,24 @@
     send_across(0)
     for i, d in enumerate(group_b):
         normalise(half + i, d)
-    units(1, 0, tiles)
-    send_back(0)
+    partner_copies[0, 1].wait_recv()
+    done = 0
+    for piece in range(pieces):
+        units(1, piece * tiles // pieces, (piece + 1) * tiles // pieces)
+        until = (piece + 1) * half // pieces
+        for i in range(done, until):
+            send_back(i)
+        done = until
     down(1)
     send_across(1)
-    send_back(1)
+    partner_copies[1, 1].wait_recv()
+    for i in range(half, n_ep):
+        send_back(i)
 
     gates = gates_ref[...]
-    mixing = jnp.where(at_first, gates[:, 0:1], 0.0) + jnp.where(at_second, gates[:, 1:2], 0.0)
+    mixing = jnp.where(at_first, column(gates[0:1]), 0.0) + jnp.where(
+        at_second, column(gates[1:2]), 0.0
+    )
     high = mixing.astype(bf16)
     low = (mixing - high.astype(f32)).astype(bf16)
     for d in range(1, n_ep):
@@ -292,9 +307,6 @@
     rows_back = back[...]
     combined = jnp.dot(high, rows_back, preferred_element_type=f32) + jnp.dot(
         low, rows_back, preferred_element_type=f32
-    )
-    diag = lax.broadcasted_iota(jnp.int32, (tok, tok), 0) == lax.broadcasted_iota(
-        jnp.int32, (tok, tok), 1
     )
     row_sum = jnp.sum(combined * combined, axis=1, keepdims=True)
     flat = jnp.sum(jnp.where(diag, row_sum, 0.0), axis=0, keepdims=True)
@@ -315,9 +327,9 @@
     for copy in norm_copies:
         copy.wait()
     total = sum(sums[j] for j in range(n_tp))
-    column = jnp.sum(jnp.where(diag, total, 0.0), axis=1, keepdims=True)
-    scale = lax.rsqrt(column / full + epsilon)
-    out_ref[...] = (combined * scale * out_gain_ref[...].astype(f32)).astype(bf16)
+    scale = lax.rsqrt(column(total) / full + epsilon)
+    gain = out_gain_ref[...].astype(f32).reshape(1, width)
+    out_ref[...] = (combined * scale * gain).astype(bf16)
 
 
 def fused(tokens, norm_gain, routes, gate_weights, w_gate, w_up, w_down, out_gain):
@@ -326,7 +338,7 @@
     cap = 2 * routes.shape[1] * tok // n_ep
     _, d_model, ff = w_gate.shape
     half_rows = n_ep // 2 * cap
-    near = (0, 2, 3, 1) + tuple(range(4, n_ep))
+    near = tuple(range(0, n_ep, 2)) + tuple(range(1, n_ep, 2))
     bf16, f32 = jnp.bfloat16, jnp.float32
     dma = pltpu.SemaphoreType.DMA
     vmem = pl.BlockSpec(memory_space=pltpu.VMEM)
@@ -365,7 +377,7 @@
             collective_id=0, has_side_effects=True, vmem_limit_bytes=60 * 1024 * 1024
         ),
     )(
-        routes, gate_weights, tokens, norm_gain.reshape(1, -1), out_gain.reshape(1, -1),
+        routes.T, gate_weights.T, tokens, norm_gain, out_gain,
         w_gate, w_up, w_down,
     )
 

time: 65.9 us -> 59.8 us (0.907); the launches traced: 65 us -> 59.7 us
  local copies, waits for them, and re-layouts: 6.88 us -> 1.57 us
    unnamed x3 -> x1, local copies, waits for them, and re-layouts: 4.38 us -> 1.57 us
    reshape x2 -> x0, local copies, waits for them, and re-layouts: 2.5 us -> none  [the longest x1 1.25 us: fused(): norm_gain.reshape(1, -1)]
where the time goes in v2:
time: 59.8 us; the launch traced here: 59.7 us
  Pallas kernels  58.1 us (97%)
  local copies, waits for them, and re-layouts  1.57 us (3%)
    pallas_call x1, Pallas kernels, fused(): pl.pallas_call(functools.partial(layer, n_ep, cap, near), out_shape=jax.S...  58.1 us
    unnamed x1, local copies, waits for them, and re-layouts  1.57 us

profile of v2, /device:TPU:0, one launch (start us, length us, event | category | flops | bytes accessed | tf_op | source)
XLA Modules:
  0.0 59.7 jit_solution(10327348370769104599)
XLA Ops:
  0.0 58.1 %shard_map.82 = bf16[128,512]{1,0:T(8,128)(2,1)} custom-call(s32[2,128]{1,0:T(2,128)} %bitcast.2, f32[2,128]{1,0:T(2,128)} %bitcast.3, bf16[128,512]{1,0:T(8,128)(2,1)} %tokens_ref.1, bf16[512]{0:T(512)(128)(2,1)} %in_gain_ref.1, bf16[512]{0:T(512)(128)(2,1)} %out_gain_ref.1, bf16[1,2048,1024]{2,1,0:T(8,128)(2,1)} %wg_hbm.1, bf16[1,2048,1024]{2,1,0:T(8,128)(2,1)} %wu_hbm.1, ...), custom_call_target="tpu_custom_call" | custom-call | tf_op jit(solution)/shard_map/pallas_call | solution.py:347
  58.1 1.6 %copy.10 = bf16[128,512]{1,0:T(8,128)(2,1)} copy(bf16[128,512]{1,0:T(8,128)(2,1)} %shard_map.82) | data formatting | bytes 262144

commit v3 on v2

--- a/solution.py
+++ b/solution.py
@@ -260,8 +260,8 @@
         copy.wait_recv()
     for i in range(1, half):
         forward(group_a[i])
-        pass_on(group_a[i - 1])
-    pass_on(group_a[half - 1])
+    for d in group_a:
+        pass_on(d)
     for i, d in enumerate(group_a):
         normalise(i, d)
     for copy in weights[:2]:

time: 59.8 us -> 59.8 us (level)
  no operation moved by 1% of the time
where the time goes in v3:
time: 59.8 us; the launch traced here: 59.7 us
  Pallas kernels  58.1 us (97%)
  local copies, waits for them, and re-layouts  1.57 us (3%)
    pallas_call x1, Pallas kernels, fused(): pl.pallas_call(functools.partial(layer, n_ep, cap, near), out_shape=jax.S...  58.1 us
    unnamed x1, local copies, waits for them, and re-layouts  1.57 us

profile of v3, /device:TPU:0, one launch (start us, length us, event | category | flops | bytes accessed | tf_op | source)
XLA Modules:
  0.0 59.7 jit_solution(17607183160198087295)
XLA Ops:
  0.0 58.1 %shard_map.82 = bf16[128,512]{1,0:T(8,128)(2,1)} custom-call(s32[2,128]{1,0:T(2,128)} %bitcast.2, f32[2,128]{1,0:T(2,128)} %bitcast.3, bf16[128,512]{1,0:T(8,128)(2,1)} %tokens_ref.1, bf16[512]{0:T(512)(128)(2,1)} %in_gain_ref.1, bf16[512]{0:T(512)(128)(2,1)} %out_gain_ref.1, bf16[1,2048,1024]{2,1,0:T(8,128)(2,1)} %wg_hbm.1, bf16[1,2048,1024]{2,1,0:T(8,128)(2,1)} %wu_hbm.1, ...), custom_call_target="tpu_custom_call" | custom-call | tf_op jit(solution)/shard_map/pallas_call | solution.py:347
  58.1 1.6 %copy.10 = bf16[128,512]{1,0:T(8,128)(2,1)} copy(bf16[128,512]{1,0:T(8,128)(2,1)} %shard_map.82) | data formatting | bytes 262144
